TPU v7x, 128 devices: a whole 4x4x4 slice. The times are simulated.
128 devices in a mesh: ra: 16 (over z, x), cb: 4 (over y), dp: 2 (over core).
Axes of the slice: x: 4, y: 4, z: 4, core: 2. Of those that a mesh axis runs over, the one named last changes fastest.
Arguments:
- tokens: bfloat16 [1024, 4096], P('dp', 'ra'), may hold values from -160 to 160, as said below
- first_gain: bfloat16 [4096], P('ra'), may hold values from 0.099609375 to 1.8984375
- first_gate: bfloat16 [4096, 6144], P('ra', 'cb'), may hold values from -0.125 to 0.125
- first_up: bfloat16 [4096, 6144], P('ra', 'cb'), may hold values from -0.125 to 0.125
- first_down: bfloat16 [6144, 4096], P(('cb', 'ra')), may hold values from -0.21875 to 0.21875
- first_branch: bfloat16 [4096], P('ra'), may hold values from 1 to 4
- second_gain: bfloat16 [4096], P('ra'), may hold values from 0.099609375 to 1.8984375
- second_gate: bfloat16 [4096, 6144], P('ra', 'cb'), may hold values from -0.125 to 0.125
- second_up: bfloat16 [4096, 6144], P('ra', 'cb'), may hold values from -0.125 to 0.125
- second_down: bfloat16 [6144, 4096], P(('cb', 'ra')), may hold values from -0.21875 to 0.21875
- second_branch: bfloat16 [4096], P('ra'), may hold values from 1 to 4
Outputs:
- mixed_out: bfloat16 [1024, 4096], P('dp', 'ra')
Inputs may be any that keep to these rules, and one draw needn't show every extreme that they name: `tokens`: activations whose scale varies by token and by feature.
All inputs are finite; a program needn't handle non-finite values.
Results may differ from a plain program's by a relative error of at most 0.035.
Values may be sent and summed in bfloat16 or wider, within the bound.
No kernel may reach another device: no remote copies, remote signals or barrier semaphores. Data moves between devices by JAX's collectives and lax.ppermute only.
A program may use at most 64 MiB of HBM per device.

v0:
```python
import jax
import jax.numpy as jnp
from jax import lax
from jax.experimental import pallas as pl
from jax.experimental.pallas import tpu as pltpu
from jax.sharding import Mesh, PartitionSpec as P

epsilon = 1e-06
residual_scale = 0.25
f32 = jnp.float32
bf16 = jnp.bfloat16
VMEM = pl.BlockSpec(memory_space=pltpu.VMEM)
SMEM = pl.BlockSpec(memory_space=pltpu.SMEM)
HBM = pl.BlockSpec(memory_space=pltpu.HBM)
ANY = pl.BlockSpec(memory_space=pl.ANY)


def exchange(x, axes):
    return lax.all_to_all(x, axes, 0, 0, tiled=True)


def other_core(x):
    return lax.ppermute(x, "dp", [(0, 1), (1, 0)])


def shifted(x, axis, step):
    return lax.ppermute(x, axis, [(i, (i + step) % 4) for i in range(4)])


def dot(a, b, dims):
    return lax.dot_general(a, b, (dims, ((), ())), preferred_element_type=f32)


def silu(v):
    return v / (1.0 + jnp.exp(-v))


def at_lane(core, half):
    return pl.ds(pl.multiple_of(core * half, 128), half)


def together(pairs, sems):
    copies = [pltpu.make_async_copy(*pair, sems.at[i]) for i, pair in enumerate(pairs)]
    for copy in copies:
        copy.start()
    return copies


def wait_for(copies):
    for copy in copies:
        copy.wait()


def pack(core_ref, z_ref, gain, tokens, gate, upward, down1, down2, *refs):
    sends, mine1, mine2, scaled, here, sems = refs[:3], refs[3], refs[4], refs[5], refs[6], refs[7]
    core, z = core_ref[0], z_ref[0]
    rows, wide = sends[0].shape
    part, half = wide // 2, mine1.shape[1]
    pairs = [(tokens, here)]
    for step, send in enumerate(sends, 1):
        at = pl.ds(pl.multiple_of(((z + step) % 4) * part, 128), part)
        for side, w in enumerate((gate, upward)):
            source = w.at[pl.ds(core * rows, rows), at]
            pairs.append((source, send.at[:, pl.ds(side * part, part)]))
    for w, mine in ((down1, mine1), (down2, mine2)):
        pairs.append((w.at[:, at_lane(core, half)], mine))
    copies = together(pairs, sems)
    copies[0].wait()
    scaled[...] = (here[...].astype(f32) * gain[...].astype(f32).reshape(1, -1)).astype(bf16)
    wait_for(copies[1:])


def message(core_ref, y_ref, branch, gain, here, tokens, gate, upward, out, picked, sems):
    core, y = core_ref[0], y_ref[0]
    width, cols = picked.shape
    each = cols // 16

    @pl.when(core == 0)
    def _():
        pltpu.make_async_copy(gate, picked, sems.at[16]).start()

    @pl.when(core == 1)
    def _():
        pltpu.make_async_copy(upward, picked, sems.at[16]).start()

    pairs = []
    for z in range(4):
        for x in range(4):
            source = tokens.at[pl.ds(x * 128 + 32 * z + 8 * y, 8), :]
            pairs.append((source, out.at[4 * z + x, pl.ds(each, 8), :]))
    copies = together(pairs, sems)
    wide = here[...].astype(f32)
    squares = lax.dot_general(
        jnp.ones((8, width), f32),
        wide * wide,
        (((1,), (1,)), ((), ())),
        precision=lax.Precision.HIGHEST,
        preferred_element_type=f32,
    )
    high = squares.astype(bf16).astype(f32)
    mid = (squares - high).astype(bf16).astype(f32)
    low = squares - high - mid
    row = lax.broadcasted_iota(jnp.int32, (8, width), 0)
    fixed = jnp.where(row == 0, branch[...].astype(f32), jnp.where(row == 1, gain[...].astype(f32), 0.0))
    blocks = []
    for x in range(4):
        at = slice(128 * x, 128 * x + 128)
        first = jnp.concatenate([high[:, at], mid[:, at]], 1)
        second = jnp.concatenate([low[:, at], jnp.zeros_like(low[:, at])], 1)
        blocks.append(jnp.where(row == 2, first, jnp.where(row == 3, second, fixed)).astype(bf16))
    pltpu.make_async_copy(gate, picked, sems.at[16]).wait()
    turned = picked[...].T
    for z in range(4):
        for x in range(4):
            to = 4 * z + x
            out[to, :each, :] = turned[to * each : (to + 1) * each, :]
            out[to, each + 8 :, :] = blocks[x]
    wait_for(copies)


def up_part(core_ref, x_ref, z_ref, first_x, gate, upward, *refs):
    xs, mine, other = refs[:3], refs[3:6], refs[6:9]
    own, sends, acc, whole, held, sems = refs[9], refs[10:13], refs[13], refs[14], refs[15], refs[16]
    core, x, z = core_ref[0], x_ref[0], z_ref[0]
    rows, wide = mine[0].shape
    part = wide // 2
    at = pl.ds(pl.multiple_of(z * part, 128), part)
    copies = [[]]
    for side, w in enumerate((gate, upward)):
        copies[0].append((w.at[:, at], whole.at[0, :, pl.ds(side * part, part)]))
    for step in range(3):
        here = (mine[step], whole.at[step + 1, pl.ds(core * rows, rows), :])
        there = (other[step], whole.at[step + 1, pl.ds((1 - core) * rows, rows), :])
        copies.append([here, there, (xs[step], held.at[step])])
    copies = [together(group, sems.at[step]) for step, group in enumerate(copies)]
    total = None
    for step in range(4):
        wait_for(copies[step])
        tokens = held[step - 1] if step else first_x[...]
        one = dot(tokens, whole[step], ((1,), (0,)))
        total = one if total is None else total + one
    acc[...] = total
    own[...] = acc[pl.ds(x * 128, 128), :]
    for step, send in enumerate(sends, 1):
        send[...] = acc[pl.ds(((x + step) % 4) * 128, 128), :].astype(bf16)


def down_part(core_ref, x_ref, own, a, b, c, side, w, *refs):
    mine, other, out, whole, small, sems = refs[:3], refs[3:6], refs[6], refs[7], refs[8], refs[9]
    core, x = core_ref[0], x_ref[0]
    rows, full = w.shape
    half = full // 2
    copies = [(side.at[:, pl.ds(rows, 16), :], small), (w, whole.at[pl.ds(x * rows, rows), :])]
    for step in range(1, 4):
        at = pl.ds(((x + 4 - step) % 4) * rows, rows)
        copies.append((mine[step - 1], whole.at[at, at_lane(core, half)]))
        copies.append((other[step - 1], whole.at[at, at_lane(1 - core, half)]))
    copies = together(copies, sems)
    both = own[...] + a[...].astype(f32) + b[...].astype(f32) + c[...].astype(f32)
    copies[0].wait()
    squares = jnp.sum(small[...].astype(f32), axis=0)[10:12]
    squares = squares[0:1, :128] + squares[0:1, 128:] + squares[1:2, :128]
    scale = lax.rsqrt(squares / full + epsilon)
    both = both * jnp.broadcast_to(scale, (8, 128)).T[:, :1]
    part = both.shape[1] // 2
    hidden = (silu(both[:, :part]) * both[:, part:]).astype(bf16)
    wait_for(copies[1:])
    out[...] = dot(hidden, whole[...], ((1,), (0,))).astype(bf16)


def join(got, side, send, small, sem):
    copy = pltpu.make_async_copy(side.at[:, pl.ds(side.shape[1] - 16, 16), :], small, sem)
    copy.start()
    total = jnp.sum(got[...].astype(f32), axis=0)
    copy.wait()
    blocks = [small[i].astype(f32) for i in range(16)]
    tokens, branch, gain = (jnp.concatenate([b[at] for b in blocks], 1) for at in (slice(0, 8), slice(8, 9), slice(9, 10)))
    middle = (residual_scale * tokens + 0.5 * branch * total).astype(bf16)
    mid = middle.astype(f32)
    square = jnp.mean(mid * mid, axis=1, keepdims=True)
    normed = (mid * lax.rsqrt(square + epsilon) * gain).astype(bf16)
    full = normed.shape[1]
    width = full // 16
    for x in range(4):
        for z in range(4):
            block = (4 * z + x) * width
            send[4 * x + z, :, :full] = normed
            send[4 * x + z, :, full:] = middle[:, block : block + width]


def finish(got, branch, send, out, middle, sems):
    count, rows = send.shape[:2]
    width = out.shape[2]
    pairs = [(send.at[:, :, pl.ds(send.shape[2] - width, width)], middle)]
    copies = together(pairs, sems)
    total = jnp.sum(got[...].astype(f32), axis=0)
    wait_for(copies)
    for j in range(count):
        at = slice(j * rows, (j + 1) * rows)
        mid = middle[j].astype(f32)
        value = (residual_scale * mid + 0.5 * branch[...].astype(f32) * total[at]).astype(bf16)
        for y in range(4):
            out[y, at, :] = value


def gated(core, tokens, sources, up, sems):
    blocks, rows, width = up.shape
    cols = rows // 8
    groups = sems.shape[0]
    each = blocks // groups
    pending = []
    for group in range(groups):
        pairs = []
        for w, first, slot, side in sources:
            begin = group * each - first
            if 0 <= begin < w.shape[0]:
                place = 1 - core if side else core
                to = up.at[pl.ds(group * each, each), pl.ds(slot * 2 * cols + place * cols, cols), :]
                pairs.append((w.at[pl.ds(begin, each), pl.ds(0, cols), :], to))
        pending.append(together(pairs, sems.at[group]))

    def finish():
        total = None
        for group in range(groups):
            wait_for(pending[group])
            for block in range(group * each, (group + 1) * each):
                part = dot(up[block], tokens[:, block * width : (block + 1) * width], ((1,), (1,)))
                total = part if total is None else total + part
        hidden = []
        for i in range(rows // (2 * cols)):
            gate = total[2 * i * cols : (2 * i + 1) * cols]
            hidden.append(silu(gate) * total[(2 * i + 1) * cols : (2 * i + 2) * cols])
        return jnp.concatenate(hidden, 0)

    return finish


def feed_forward(core_ref, got, w_down, *refs):
    ups, mine, other, out = refs[:14], refs[14:17], refs[17:20], refs[20]
    tokens, up, whole, up_sems, down_sems = refs[21:]
    core = core_ref[0]
    rows, full = w_down.shape
    half = full // 2
    blocks, _, width = up.shape
    sources = [(ups[0], 0, 0, 0), (ups[1], 0, 0, 1)]
    for i, w in enumerate(ups[2:]):
        sources.append((w, blocks // 2 * (i // 2 % 2), 1 + i // 4, i % 2))
    finish = gated(core, tokens, sources, up, up_sems)
    pairs = [(w_down, whole.at[pl.ds(0, rows), :])]
    for step in range(1, 4):
        at = pl.ds(step * rows, rows)
        pairs.append((mine[step - 1], whole.at[at, at_lane(core, half)]))
        pairs.append((other[step - 1], whole.at[at, at_lane(1 - core, half)]))
    copies = together(pairs, down_sems)
    for j in range(got.shape[0]):
        tokens[8 * j : 8 * j + 8, :] = got[j, :, :full]
    hidden = finish().T.astype(bf16)
    wait_for(copies)
    for block in range(blocks):
        lanes = slice(block * width, (block + 1) * width)
        out[block] = dot(hidden, whole[:, lanes], ((1,), (0,))).astype(bf16)


def shards(
    tokens,
    first_gain,
    first_gate,
    first_up,
    first_down,
    first_branch,
    second_gain,
    second_gate,
    second_up,
    second_down,
    second_branch,
):
    core, x, y, z = (lax.axis_index(name) for name in ("dp", "rx", "cb", "rz"))
    core_ref, x_ref, y_ref, z_ref = (i.astype(jnp.int32).reshape(1) for i in (core, x, y, z))
    n_tok, width = tokens.shape
    full = width * 16
    half = width // 2
    cols = first_gate.shape[1]
    part = cols // 4
    few = n_tok // 4
    w_half = jax.ShapeDtypeStruct((first_down.shape[0], full // 2), bf16)

    def kernel(body, ins, *outs, scratch=(), mib=16):
        call = pl.pallas_call(
            body,
            out_shape=list(outs) if len(outs) > 1 else outs[0],
            in_specs=ins,
            out_specs=[VMEM] * len(outs) if len(outs) > 1 else VMEM,
            scratch_shapes=list(scratch),
            compiler_params=pltpu.CompilerParams(vmem_limit_bytes=mib * 2**20),
        )

        def run(*args):
            kept = [pltpu.with_memory_space_constraint(a, pltpu.HBM) if spec is HBM else a for a, spec in zip(args, ins)]
            return call(*kept)

        return run

    dma = pltpu.SemaphoreType.DMA

    *w1, d1, d2, scaled = kernel(
        pack,
        [SMEM] * 2 + [VMEM] + [HBM] * 5,
        *[jax.ShapeDtypeStruct((half, 2 * part), bf16)] * 3,
        w_half,
        w_half,
        jax.ShapeDtypeStruct(tokens.shape, bf16),
        scratch=[pltpu.VMEM(tokens.shape, bf16), dma((9,))],
    )(core_ref, z_ref, first_gain, tokens, first_gate, first_up, first_down, second_down)
    w1 = [shifted(w, "rz", step) for step, w in enumerate(w1, 1)]
    x1 = [scaled] + [shifted(scaled, "rz", step) for step in (1, 2, 3)]
    w1_other = [other_core(w) for w in w1]

    side = kernel(
        message,
        [SMEM] * 2 + [VMEM] * 3 + [HBM] * 3,
        jax.ShapeDtypeStruct((16, cols // 16 + 16, width), bf16),
        scratch=[pltpu.VMEM((width, cols), bf16), dma((17,))],
    )(core_ref, y_ref, first_branch[None], second_gain[None], tokens, tokens, second_gate, second_up)
    side = exchange(side, ("rz", "rx"))
    d1 = [shifted(d1, "rx", step) for step in (1, 2, 3)]
    d2 = [shifted(d2, "cb", step) for step in (1, 2, 3)]
    d1_other = [other_core(w) for w in d1]
    d2_other = [other_core(w) for w in d2]

    def swapped(ws):
        return [other_core(w) for w in ws]

    low, high = side[:8, : cols // 16], side[8:, : cols // 16]
    low = [shifted(low, "cb", step) for step in (1, 3)]
    high = [shifted(high, "cb", step) for step in (1, 3)]
    far = [shifted(low[0], "cb", 1)]
    far += [shifted(high[1], "cb", 3)]
    own_other, *low_other = swapped([side, *low])
    high_other = swapped(high)
    far_other = swapped(far)
    v1 = [side, own_other, low[0], low_other[0], high[0], high_other[0]]
    v1 += [far[0], far_other[0], far[1], far_other[1], low[1], low_other[1], high[1], high_other[1]]

    own, *sends = kernel(
        up_part,
        [SMEM] * 3 + [VMEM] + [HBM] * 11,
        jax.ShapeDtypeStruct((few, 2 * part), f32),
        *[jax.ShapeDtypeStruct((few, 2 * part), bf16)] * 3,
        scratch=[
            pltpu.VMEM((n_tok, 2 * part), f32),
            pltpu.VMEM((4, width, 2 * part), bf16),
            pltpu.VMEM((3, n_tok, width), bf16),
            dma((4, 3)),
        ],
    )(core_ref, x_ref, z_ref, x1[0], first_gate, first_up, *x1[1:], *w1, *w1_other)
    got = [shifted(send, "rx", step) for step, send in enumerate(sends, 1)]
    partial = kernel(
        down_part,
        [SMEM] * 2 + [VMEM] * 4 + [HBM] * 8,
        pltpu.VMEM((few, full), bf16),
        scratch=[pltpu.VMEM((part, full), bf16), pltpu.VMEM((16, 16, width), bf16), dma((8,))],
    )(core_ref, x_ref, own, *got, side, first_down, *d1, *d1_other)
    got = exchange(partial.reshape(16, 8, full), ("rz", "cb"))
    send = kernel(
        join,
        [VMEM, HBM],
        jax.ShapeDtypeStruct((16, 8, full + width), bf16),
        scratch=[pltpu.VMEM((16, 16, width), bf16), dma(())],
    )(got, side)
    rows = exchange(send, ("rx", "rz"))
    partial = kernel(
        feed_forward,
        [SMEM, VMEM] + [HBM] * 2 + [ANY] + [HBM] * 18,
        pltpu.VMEM((16, few, width), bf16),
        scratch=[
            pltpu.VMEM((few, full), bf16),
            pltpu.VMEM((16, 2 * part, width), bf16),
            pltpu.VMEM((part, full), bf16),
            dma((4, 8)),
            dma((7,)),
        ],
        mib=24,
    )(core_ref, rows, second_down, *v1, *d2, *d2_other)
    partial, branch = lax.optimization_barrier((partial, second_branch[None]))
    got = exchange(partial, ("rz", "rx"))
    out = kernel(
        finish,
        [VMEM, VMEM, HBM],
        pltpu.VMEM((4, few, width), bf16),
        scratch=[pltpu.VMEM((16, 8, width), bf16), dma((1,))],
    )(got, branch, rows)
    out = exchange(out, "cb")
    return out.reshape(4, 16, 8, width).transpose(1, 0, 2, 3).reshape(n_tok, width)


def solution(mesh):
    fine = Mesh(mesh.devices.reshape(4, 4, 4, 2), ("rz", "rx", "cb", "dp"))
    ra = ("rz", "rx")
    vector, up, dn = P(ra), P(ra, "cb"), P(("cb", *ra), None)
    layer = (vector, up, up, dn, vector)
    return jax.shard_map(
        shards,
        mesh=fine,
        in_specs=(P("dp", ra), *layer, *layer),
        out_specs=P("dp", ra),
        check_vma=False,
    )
```

profile of v0, /device:TPU:0, one launch (start us, length us, event | category | flops | bytes accessed | tf_op | source)
XLA Modules:
  0.0 189.1 jit_solution(18092771165497835559)
XLA Ops:
  11.1 3.5 %shard_map.111 = bf16[16,112,256]{2,1,0:T(8,128)(2,1)} custom-call(s32[1]{0:T(128)} %bitcast.core_ref, s32[1]{0:T(128)} %bitcast.3.y_ref, bf16[1,256]{1,0:T(2,128)(2,1)S(1)} %broadcast_in_dim.9.branch, bf16[1,256]{1,0:T(2,128)(2,1)S(1)} %broadcast_in_dim.10.gain, bf16[512,256]{1,0:T(8,128)(2,1)} %tokens.3, bf16[512,256]{1,0:T(8,128)(2,1)} %tokens.3, ...), custom_call_target="tpu_custom_call" | custom-call | tf_op jit(solution)/shard_map/pallas_call | solution.py:299
  14.6 6.2 %all-to-all-start = ((bf16[16,112,256]{2,1,0:T(8,128)(2,1)}), bf16[16,112,256]{2,1,0:T(8,128)(2,1)S(1)}, u32[]{:S(2)}, u32[]{:S(2)}) async-start(bf16[16,112,256]{2,1,0:T(8,128)(2,1)} %shard_map.111), calls=%async_computation | async-start | bytes 1835008 | tf_op jit(solution)/shard_map/all_to_all | solution.py:19
  20.9 3.2 %collective-permute-start.2 = (bf16[512,256]{1,0:T(8,128)(2,1)S(1)}, bf16[512,256]{1,0:T(8,128)(2,1)S(1)}, u32[]{:S(2)}, u32[]{:S(2)}) collective-permute-start(bf16[512,256]{1,0:T(8,128)(2,1)S(1)} %get-tuple-element.17.first_x), channel_id=1, source_target_pairs={{0,96},{32,0},{64,32},{96,64},{1,97},{33,1},{65,33},{97,65},{2,98}... | collective-permute-start | bytes 786440 | tf_op jit(solution)/shard_map/ppermute | solution.py:27
  24.1 12.4 %collective-permute-done.4.refs_4_ = bf16[128,768]{1,0:T(8,128)(2,1)S(1)} collective-permute-done((bf16[128,768]{1,0:T(8,128)(2,1)S(1)}, bf16[128,768]{1,0:T(8,128)(2,1)S(1)}, u32[]{:S(2)}, u32[]{:S(2)}) %collective-permute-start.4) | collective-permute-done | bytes 196640 | tf_op jit(solution)/shard_map/ppermute | solution.py:27
  38.4 2.5 %collective-permute-start.13 = (bf16[96,2048]{1,0:T(8,128)(2,1)S(1)}, bf16[96,2048]{1,0:T(8,128)(2,1)S(1)}, u32[]{:S(2)}, u32[]{:S(2)}) collective-permute-start(bf16[96,2048]{1,0:T(8,128)(2,1)S(1)} %get-tuple-element.25), channel_id=1, source_target_pairs={{0,16},{8,24},{16,0},{24,8},{1,17},{9,25},{17,1},{25,9},{2,18},{10... | collective-permute-start | bytes 1179656 | tf_op jit(solution)/shard_map/ppermute | solution.py:27
  45.4 2.8 %shard_map.110 = (f32[128,768]{1,0:T(8,128)S(1)}, bf16[128,768]{1,0:T(8,128)(2,1)S(1)}, bf16[128,768]{1,0:T(8,128)(2,1)S(1)}, bf16[128,768]{1,0:T(8,128)(2,1)S(1)}) custom-call(s32[1]{0:T(128)} %bitcast.core_ref, s32[1]{0:T(128)} %bitcast.1.x_ref, s32[1]{0:T(128)} %bitcast.2.z_ref, bf16[512,256]{1,0:T(8,128)(2,1)S(1)} %get-tuple-element.17.first_x, ...), custom_call_target="tpu_custom_call" | custom-call | tf_op jit(solution)/shard_map/pallas_call | solution.py:299
  49.2 10.0 %collective-permute-done.13.refs_1_ = bf16[96,2048]{1,0:T(8,128)(2,1)S(1)} collective-permute-done((bf16[96,2048]{1,0:T(8,128)(2,1)S(1)}, bf16[96,2048]{1,0:T(8,128)(2,1)S(1)}, u32[]{:S(2)}, u32[]{:S(2)}) %collective-permute-start.13) | collective-permute-done | bytes 393248 | tf_op jit(solution)/shard_map/ppermute | solution.py:27
  63.0 2.2 %collective-permute-start.9 = (bf16[128,768]{1,0:T(8,128)(2,1)S(1)}, bf16[128,768]{1,0:T(8,128)(2,1)S(1)}, u32[]{:S(2)}, u32[]{:S(2)}) collective-permute-start(bf16[128,768]{1,0:T(8,128)(2,1)S(1)} %get-tuple-element.22), channel_id=1, source_target_pairs={{0,8},{8,16},{16,24},{24,0},{1,9},{9,17},{17,25},{25,1},{2,10},{10... | collective-permute-start | bytes 589832 | tf_op jit(solution)/shard_map/ppermute | solution.py:27
  66.7 3.8 %collective-permute-done.9.a = bf16[128,768]{1,0:T(8,128)(2,1)S(1)} collective-permute-done((bf16[128,768]{1,0:T(8,128)(2,1)S(1)}, bf16[128,768]{1,0:T(8,128)(2,1)S(1)}, u32[]{:S(2)}, u32[]{:S(2)}) %collective-permute-start.9) | collective-permute-done | bytes 196640 | tf_op jit(solution)/shard_map/ppermute | solution.py:27
  73.1 3.7 %shard_map.112 = bf16[128,4096]{1,0:T(8,128)(2,1)} custom-call(s32[1]{0:T(128)} %bitcast.core_ref, s32[1]{0:T(128)} %bitcast.1.x_ref, f32[128,768]{1,0:T(8,128)S(1)} %get-tuple-element.21.own, bf16[128,768]{1,0:T(8,128)(2,1)S(1)} %collective-permute-done.9.a, bf16[128,768]{1,0:T(8,128)(2,1)S(1)} %collective-permute-done.10.b, ...), custom_call_target="tpu_custom_call" | custom-call | tf_op jit(solution)/shard_map/pallas_call | solution.py:299
  76.8 4.7 %all-to-all-start.1 = ((bf16[16,8,4096]{2,1,0:T(8,128)(2,1)}), bf16[16,8,4096]{2,1,0:T(8,128)(2,1)S(1)}, u32[]{:S(2)}, u32[]{:S(2)}) async-start(bf16[16,8,4096]{2,1,0:T(8,128)(2,1)} %bitcast.4), calls=%async_computation.1 | async-start | bytes 2097152 | tf_op jit(solution)/shard_map/all_to_all | solution.py:19
  83.4 2.7 %collective-permute-start.32 = (bf16[96,2048]{1,0:T(8,128)(2,1)S(1)}, bf16[96,2048]{1,0:T(8,128)(2,1)S(1)}, u32[]{:S(2)}, u32[]{:S(2)}) collective-permute-start(bf16[96,2048]{1,0:T(8,128)(2,1)S(1)} %get-tuple-element.26), channel_id=1, source_target_pairs={{0,4},{2,6},{4,0},{6,2},{1,5},{3,7},{5,1},{7,3},{8,12},{10,14},{12... | collective-permute-start | bytes 1179656 | tf_op jit(solution)/shard_map/ppermute | solution.py:27
  87.6 18.1 %collective-permute-done.31.refs_14_ = bf16[96,2048]{1,0:T(8,128)(2,1)S(1)} collective-permute-done((bf16[96,2048]{1,0:T(8,128)(2,1)S(1)}, bf16[96,2048]{1,0:T(8,128)(2,1)S(1)}, u32[]{:S(2)}, u32[]{:S(2)}) %collective-permute-start.31) | collective-permute-done | bytes 393248 | tf_op jit(solution)/shard_map/ppermute | solution.py:27
  105.7 6.6 %collective-permute-done.32.refs_15_ = bf16[96,2048]{1,0:T(8,128)(2,1)S(1)} collective-permute-done((bf16[96,2048]{1,0:T(8,128)(2,1)S(1)}, bf16[96,2048]{1,0:T(8,128)(2,1)S(1)}, u32[]{:S(2)}, u32[]{:S(2)}) %collective-permute-start.32) | collective-permute-done | bytes 393248 | tf_op jit(solution)/shard_map/ppermute | solution.py:27
  113.8 3.2 %collective-permute-start.25 = (bf16[8,96,256]{2,1,0:T(8,128)(2,1)}, bf16[8,96,256]{2,1,0:T(8,128)(2,1)}, u32[]{:S(2)}, u32[]{:S(2)}) collective-permute-start(bf16[8,96,256]{2,1,0:T(8,128)(2,1)} %get-tuple-element.29), channel_id=1, source_target_pairs={{0,6},{2,0},{4,2},{6,4},{1,7},{3,1},{5,3},{7,5},{8,14},{10,8},{12,... | collective-permute-start | bytes 1179656 | tf_op jit(solution)/shard_map/ppermute | solution.py:27
  118.5 2.5 %collective-permute-start.28 = (bf16[8,96,256]{2,1,0:T(8,128)(2,1)}, bf16[8,96,256]{2,1,0:T(8,128)(2,1)}, u32[]{:S(2)}, u32[]{:S(2)}) collective-permute-start(bf16[8,96,256]{2,1,0:T(8,128)(2,1)} %get-tuple-element.30), channel_id=1, source_target_pairs={{0,6},{2,0},{4,2},{6,4},{1,7},{3,1},{5,3},{7,5},{8,14},{10,8},{12,... | collective-permute-start | bytes 1179656 | tf_op jit(solution)/shard_map/ppermute | solution.py:27
  121.0 2.2 %shard_map.113 = bf16[16,8,4352]{2,1,0:T(8,128)(2,1)} custom-call(bf16[16,8,4096]{2,1,0:T(8,128)(2,1)S(1)} %all-to-all-done.1.got, bf16[16,112,256]{2,1,0:T(8,128)(2,1)} %copy-done.2), custom_call_target="tpu_custom_call" | custom-call | tf_op jit(solution)/shard_map/pallas_call | solution.py:299
  123.2 5.5 %all-to-all-start.2 = ((bf16[16,8,4352]{2,1,0:T(8,128)(2,1)}), bf16[16,8,4352]{2,1,0:T(8,128)(2,1)S(1)}, u32[]{:S(2)}, u32[]{:S(2)}) async-start(bf16[16,8,4352]{2,1,0:T(8,128)(2,1)} %shard_map.113), calls=%async_computation.2 | async-start | bytes 2228224 | tf_op jit(solution)/shard_map/all_to_all | solution.py:19
  129.0 3.2 %collective-permute-start.26 = (bf16[8,96,256]{2,1,0:T(8,128)(2,1)}, bf16[8,96,256]{2,1,0:T(8,128)(2,1)S(1)}, u32[]{:S(2)}, u32[]{:S(2)}) collective-permute-start(bf16[8,96,256]{2,1,0:T(8,128)(2,1)} %collective-permute-done.25.refs_12_), channel_id=1, source_target_pairs={{0,6},{2,0},{4,2},{6,4},{1,7},{3,1},{5,3},{7,5},{8,14},{10,8},{12,... | collective-permute-start | bytes 1179656 | tf_op jit(solution)/shard_map/ppermute | solution.py:27
  132.2 3.5 %collective-permute-done.21.refs_4_ = bf16[8,96,256]{2,1,0:T(8,128)(2,1)} collective-permute-done((bf16[8,96,256]{2,1,0:T(8,128)(2,1)}, bf16[8,96,256]{2,1,0:T(8,128)(2,1)}, u32[]{:S(2)}, u32[]{:S(2)}) %collective-permute-start.21) | collective-permute-done | bytes 393248 | tf_op jit(solution)/shard_map/ppermute | solution.py:27
  136.2 6.9 %collective-permute-done.23.refs_6_ = bf16[8,96,256]{2,1,0:T(8,128)(2,1)S(1)} collective-permute-done((bf16[8,96,256]{2,1,0:T(8,128)(2,1)}, bf16[8,96,256]{2,1,0:T(8,128)(2,1)S(1)}, u32[]{:S(2)}, u32[]{:S(2)}) %collective-permute-start.23) | collective-permute-done | bytes 393248 | tf_op jit(solution)/shard_map/ppermute | solution.py:27
  147.2 6.7 %shard_map.114 = bf16[16,128,256]{2,1,0:T(8,128)(2,1)S(1)} custom-call(s32[1]{0:T(128)} %bitcast.core_ref, bf16[16,8,4352]{2,1,0:T(8,128)(2,1)S(1)} %all-to-all-done.2.got.send, bf16[96,4096]{1,0:T(8,128)(2,1)} %w_down.1, bf16[16,112,256]{2,1,0:T(8,128)(2,1)} %copy-done.2, bf16[16,112,256]{2,1,0:T(8,128)(2,1)S(1)} %collective-permute-done.18.refs_1_, ...), custom_call_target="tpu_custom_call" | custom-call | tf_op jit(solution)/shard_map/pallas_call | solution.py:299
  153.9 23.2 %all_to_all.25.got = bf16[16,128,256]{2,1,0:T(8,128)(2,1)S(1)} all-to-all(bf16[16,128,256]{2,1,0:T(8,128)(2,1)S(1)} %shard_map.114), channel_id=1, replica_groups=mesh['rz'=4,'rx'=4,'cb'=4,'dp'=2] {'rz','rx'}, dimensions={0} | all-to-all | bytes 2097152 | tf_op jit(solution)/shard_map/all_to_all | solution.py:19
  178.0 10.4 %all_to_all.26 = bf16[4,128,256]{2,1,0:T(8,128)(2,1)S(1)} all-to-all(bf16[4,128,256]{2,1,0:T(8,128)(2,1)S(1)} %shard_map.115), channel_id=1, replica_groups=mesh['rz'=4,'rx'=4,'cb'=4,'dp'=2] {'cb'}, dimensions={0} | all-to-all | bytes 524288 | tf_op jit(solution)/shard_map/all_to_all | solution.py:19
  (128 shorter events, 38.9 us)
Async XLA Ops:
  2.2 18.6 %collective-permute-start.3 = (bf16[128,768]{1,0:T(8,128)(2,1)S(1)}, bf16[128,768]{1,0:T(8,128)(2,1)S(1)}, u32[]{:S(2)}, u32[]{:S(2)}) collective-permute-start(bf16[128,768]{1,0:T(8,128)(2,1)S(1)} %get-tuple-element.18), channel_id=1, source_target_pairs={{0,32},{32,64},{64,96},{96,0},{1,33},{33,65},{65,97},{97,1},{2,34}... | collective-permute-start | bytes 589832 | tf_op jit(solution)/shard_map/ppermute | solution.py:27
  4.3 34.1 %collective-permute-start = (bf16[512,256]{1,0:T(8,128)(2,1)S(1)}, bf16[512,256]{1,0:T(8,128)(2,1)}, u32[]{:S(2)}, u32[]{:S(2)}) collective-permute-start(bf16[512,256]{1,0:T(8,128)(2,1)S(1)} %get-tuple-element.17.first_x), channel_id=1, source_target_pairs={{0,32},{32,64},{64,96},{96,0},{1,33},{33,65},{65,97},{97,1},{2,34}... | collective-permute-start | bytes 786440 | tf_op jit(solution)/shard_map/ppermute | solution.py:27
  6.2 34.7 %collective-permute-start.1 = (bf16[512,256]{1,0:T(8,128)(2,1)S(1)}, bf16[512,256]{1,0:T(8,128)(2,1)}, u32[]{:S(2)}, u32[]{:S(2)}) collective-permute-start(bf16[512,256]{1,0:T(8,128)(2,1)S(1)} %get-tuple-element.17.first_x), channel_id=1, source_target_pairs={{0,64},{32,96},{64,0},{96,32},{1,65},{33,97},{65,1},{97,33},{2,66}... | collective-permute-start | bytes 786440 | tf_op jit(solution)/shard_map/ppermute | solution.py:27
  8.0 28.5 %collective-permute-start.4 = (bf16[128,768]{1,0:T(8,128)(2,1)S(1)}, bf16[128,768]{1,0:T(8,128)(2,1)S(1)}, u32[]{:S(2)}, u32[]{:S(2)}) collective-permute-start(bf16[128,768]{1,0:T(8,128)(2,1)S(1)} %get-tuple-element.19), channel_id=1, source_target_pairs={{0,64},{32,96},{64,0},{96,32},{1,65},{33,97},{65,1},{97,33},{2,66}... | collective-permute-start | bytes 589832 | tf_op jit(solution)/shard_map/ppermute | solution.py:27
  9.8 26.8 %collective-permute-start.5 = (bf16[128,768]{1,0:T(8,128)(2,1)S(1)}, bf16[128,768]{1,0:T(8,128)(2,1)S(1)}, u32[]{:S(2)}, u32[]{:S(2)}) collective-permute-start(bf16[128,768]{1,0:T(8,128)(2,1)S(1)} %get-tuple-element.20), channel_id=1, source_target_pairs={{0,96},{32,0},{64,32},{96,64},{1,97},{33,1},{65,33},{97,65},{2,98}... | collective-permute-start | bytes 589832 | tf_op jit(solution)/shard_map/ppermute | solution.py:27
  14.6 57.5 %all-to-all-start = ((bf16[16,112,256]{2,1,0:T(8,128)(2,1)}), bf16[16,112,256]{2,1,0:T(8,128)(2,1)S(1)}, u32[]{:S(2)}, u32[]{:S(2)}) async-start(bf16[16,112,256]{2,1,0:T(8,128)(2,1)} %shard_map.111), calls=%async_computation | async-start | bytes 1835008 | tf_op jit(solution)/shard_map/all_to_all | solution.py:19
  20.9 21.4 %collective-permute-start.2 = (bf16[512,256]{1,0:T(8,128)(2,1)S(1)}, bf16[512,256]{1,0:T(8,128)(2,1)S(1)}, u32[]{:S(2)}, u32[]{:S(2)}) collective-permute-start(bf16[512,256]{1,0:T(8,128)(2,1)S(1)} %get-tuple-element.17.first_x), channel_id=1, source_target_pairs={{0,96},{32,0},{64,32},{96,64},{1,97},{33,1},{65,33},{97,65},{2,98}... | collective-permute-start | bytes 786440 | tf_op jit(solution)/shard_map/ppermute | solution.py:27
  38.4 20.8 %collective-permute-start.13 = (bf16[96,2048]{1,0:T(8,128)(2,1)S(1)}, bf16[96,2048]{1,0:T(8,128)(2,1)S(1)}, u32[]{:S(2)}, u32[]{:S(2)}) collective-permute-start(bf16[96,2048]{1,0:T(8,128)(2,1)S(1)} %get-tuple-element.25), channel_id=1, source_target_pairs={{0,16},{8,24},{16,0},{24,8},{1,17},{9,25},{17,1},{25,9},{2,18},{10... | collective-permute-start | bytes 1179656 | tf_op jit(solution)/shard_map/ppermute | solution.py:27
  40.9 18.4 %collective-permute-start.14 = (bf16[96,2048]{1,0:T(8,128)(2,1)S(1)}, bf16[96,2048]{1,0:T(8,128)(2,1)}, u32[]{:S(2)}, u32[]{:S(2)}) collective-permute-start(bf16[96,2048]{1,0:T(8,128)(2,1)S(1)} %get-tuple-element.25), channel_id=1, source_target_pairs={{0,24},{8,0},{16,8},{24,16},{1,25},{9,1},{17,9},{25,17},{2,26},{10... | collective-permute-start | bytes 1179656 | tf_op jit(solution)/shard_map/ppermute | solution.py:27
  48.2 14.8 %collective-permute-start.10 = (bf16[128,768]{1,0:T(8,128)(2,1)S(1)}, bf16[128,768]{1,0:T(8,128)(2,1)S(1)}, u32[]{:S(2)}, u32[]{:S(2)}) collective-permute-start(bf16[128,768]{1,0:T(8,128)(2,1)S(1)} %get-tuple-element.23), channel_id=1, source_target_pairs={{0,16},{8,24},{16,0},{24,8},{1,17},{9,25},{17,1},{25,9},{2,18},{10... | collective-permute-start | bytes 589832 | tf_op jit(solution)/shard_map/ppermute | solution.py:27
  49.2 21.3 %collective-permute-start.15 = (bf16[96,2048]{1,0:T(8,128)(2,1)S(1)}, bf16[96,2048]{1,0:T(8,128)(2,1)S(1)}, u32[]{:S(2)}, u32[]{:S(2)}) collective-permute-start(bf16[96,2048]{1,0:T(8,128)(2,1)S(1)} %collective-permute-done.12.refs_0_), channel_id=1, source_target_pairs={{0,1},{1,0},{2,3},{3,2},{4,5},{5,4},{6,7},{7,6},{8,9},{9,8},{10,11... | collective-permute-start | bytes 1179656 | tf_op jit(solution)/shard_map/ppermute | solution.py:23
  76.8 44.2 %all-to-all-start.1 = ((bf16[16,8,4096]{2,1,0:T(8,128)(2,1)}), bf16[16,8,4096]{2,1,0:T(8,128)(2,1)S(1)}, u32[]{:S(2)}, u32[]{:S(2)}) async-start(bf16[16,8,4096]{2,1,0:T(8,128)(2,1)} %bitcast.4), calls=%async_computation.1 | async-start | bytes 2097152 | tf_op jit(solution)/shard_map/all_to_all | solution.py:19
  81.5 24.2 %collective-permute-start.31 = (bf16[96,2048]{1,0:T(8,128)(2,1)S(1)}, bf16[96,2048]{1,0:T(8,128)(2,1)S(1)}, u32[]{:S(2)}, u32[]{:S(2)}) collective-permute-start(bf16[96,2048]{1,0:T(8,128)(2,1)S(1)} %get-tuple-element.26), channel_id=1, source_target_pairs={{0,2},{2,4},{4,6},{6,0},{1,3},{3,5},{5,7},{7,1},{8,10},{10,12},{12... | collective-permute-start | bytes 1179656 | tf_op jit(solution)/shard_map/ppermute | solution.py:27
  83.4 28.8 %collective-permute-start.32 = (bf16[96,2048]{1,0:T(8,128)(2,1)S(1)}, bf16[96,2048]{1,0:T(8,128)(2,1)S(1)}, u32[]{:S(2)}, u32[]{:S(2)}) collective-permute-start(bf16[96,2048]{1,0:T(8,128)(2,1)S(1)} %get-tuple-element.26), channel_id=1, source_target_pairs={{0,4},{2,6},{4,0},{6,2},{1,5},{3,7},{5,1},{7,3},{8,12},{10,14},{12... | collective-permute-start | bytes 1179656 | tf_op jit(solution)/shard_map/ppermute | solution.py:27
  86.1 26.2 %collective-permute-start.33 = (bf16[96,2048]{1,0:T(8,128)(2,1)S(1)}, bf16[96,2048]{1,0:T(8,128)(2,1)}, u32[]{:S(2)}, u32[]{:S(2)}) collective-permute-start(bf16[96,2048]{1,0:T(8,128)(2,1)S(1)} %get-tuple-element.26), channel_id=1, source_target_pairs={{0,6},{2,0},{4,2},{6,4},{1,7},{3,1},{5,3},{7,5},{8,14},{10,8},{12,... | collective-permute-start | bytes 1179656 | tf_op jit(solution)/shard_map/ppermute | solution.py:27
  112.3 16.5 %collective-permute-start.36 = (bf16[96,2048]{1,0:T(8,128)(2,1)}, bf16[96,2048]{1,0:T(8,128)(2,1)}, u32[]{:S(2)}, u32[]{:S(2)}) collective-permute-start(bf16[96,2048]{1,0:T(8,128)(2,1)} %collective-permute-done.33.refs_16_), channel_id=1, source_target_pairs={{0,1},{1,0},{2,3},{3,2},{4,5},{5,4},{6,7},{7,6},{8,9},{9,8},{10,11... | collective-permute-start | bytes 1179656 | tf_op jit(solution)/shard_map/ppermute | solution.py:23
  113.8 15.1 %collective-permute-start.19 = (bf16[8,96,256]{2,1,0:T(8,128)(2,1)}, bf16[8,96,256]{2,1,0:T(8,128)(2,1)}, u32[]{:S(2)}, u32[]{:S(2)}) collective-permute-start(bf16[8,96,256]{2,1,0:T(8,128)(2,1)} %get-tuple-element.30), channel_id=1, source_target_pairs={{0,2},{2,4},{4,6},{6,0},{1,3},{3,5},{5,7},{7,1},{8,10},{10,12},{12... | collective-permute-start | bytes 1179656 | tf_op jit(solution)/shard_map/ppermute | solution.py:27
  113.8 15.2 %collective-permute-start.25 = (bf16[8,96,256]{2,1,0:T(8,128)(2,1)}, bf16[8,96,256]{2,1,0:T(8,128)(2,1)}, u32[]{:S(2)}, u32[]{:S(2)}) collective-permute-start(bf16[8,96,256]{2,1,0:T(8,128)(2,1)} %get-tuple-element.29), channel_id=1, source_target_pairs={{0,6},{2,0},{4,2},{6,4},{1,7},{3,1},{5,3},{7,5},{8,14},{10,8},{12,... | collective-permute-start | bytes 1179656 | tf_op jit(solution)/shard_map/ppermute | solution.py:27
  117.0 18.7 %collective-permute-start.21 = (bf16[8,96,256]{2,1,0:T(8,128)(2,1)}, bf16[8,96,256]{2,1,0:T(8,128)(2,1)}, u32[]{:S(2)}, u32[]{:S(2)}) collective-permute-start(bf16[8,96,256]{2,1,0:T(8,128)(2,1)} %get-tuple-element.29), channel_id=1, source_target_pairs={{0,2},{2,4},{4,6},{6,0},{1,3},{3,5},{5,7},{7,1},{8,10},{10,12},{12... | collective-permute-start | bytes 1179656 | tf_op jit(solution)/shard_map/ppermute | solution.py:27
  118.5 17.2 %collective-permute-start.28 = (bf16[8,96,256]{2,1,0:T(8,128)(2,1)}, bf16[8,96,256]{2,1,0:T(8,128)(2,1)}, u32[]{:S(2)}, u32[]{:S(2)}) collective-permute-start(bf16[8,96,256]{2,1,0:T(8,128)(2,1)} %get-tuple-element.30), channel_id=1, source_target_pairs={{0,6},{2,0},{4,2},{6,4},{1,7},{3,1},{5,3},{7,5},{8,14},{10,8},{12,... | collective-permute-start | bytes 1179656 | tf_op jit(solution)/shard_map/ppermute | solution.py:27
  123.2 23.9 %all-to-all-start.2 = ((bf16[16,8,4352]{2,1,0:T(8,128)(2,1)}), bf16[16,8,4352]{2,1,0:T(8,128)(2,1)S(1)}, u32[]{:S(2)}, u32[]{:S(2)}) async-start(bf16[16,8,4352]{2,1,0:T(8,128)(2,1)} %shard_map.113), calls=%async_computation.2 | async-start | bytes 2228224 | tf_op jit(solution)/shard_map/all_to_all | solution.py:19
  128.8 16.9 %collective-permute-start.18 = (bf16[16,112,256]{2,1,0:T(8,128)(2,1)S(1)}, bf16[16,112,256]{2,1,0:T(8,128)(2,1)S(1)}, u32[]{:S(2)}, u32[]{:S(2)}) collective-permute-start(bf16[16,112,256]{2,1,0:T(8,128)(2,1)S(1)} %copy-done.4), channel_id=1, source_target_pairs={{0,1},{1,0},{2,3},{3,2},{4,5},{5,4},{6,7},{7,6},{8,9},{9,8},{10,11... | collective-permute-start | bytes 2752520 | tf_op jit(solution)/shard_map/ppermute | solution.py:23
  128.9 14.2 %collective-permute-start.23 = (bf16[8,96,256]{2,1,0:T(8,128)(2,1)}, bf16[8,96,256]{2,1,0:T(8,128)(2,1)S(1)}, u32[]{:S(2)}, u32[]{:S(2)}) collective-permute-start(bf16[8,96,256]{2,1,0:T(8,128)(2,1)} %collective-permute-done.19.refs_2_), channel_id=1, source_target_pairs={{0,2},{2,4},{4,6},{6,0},{1,3},{3,5},{5,7},{7,1},{8,10},{10,12},{12... | collective-permute-start | bytes 1179656 | tf_op jit(solution)/shard_map/ppermute | solution.py:27
  129.0 14.2 %collective-permute-start.26 = (bf16[8,96,256]{2,1,0:T(8,128)(2,1)}, bf16[8,96,256]{2,1,0:T(8,128)(2,1)S(1)}, u32[]{:S(2)}, u32[]{:S(2)}) collective-permute-start(bf16[8,96,256]{2,1,0:T(8,128)(2,1)} %collective-permute-done.25.refs_12_), channel_id=1, source_target_pairs={{0,6},{2,0},{4,2},{6,4},{1,7},{3,1},{5,3},{7,5},{8,14},{10,8},{12,... | collective-permute-start | bytes 1179656 | tf_op jit(solution)/shard_map/ppermute | solution.py:27
  (45 other events, 317.9 us)
where the time goes:
time: 190 us; the launch traced here: 189 us
  waiting for transfers between devices  66.7 us (35%)
  starting transfers between devices  57 us (30%)
  blocking collectives  33.6 us (18%)
  Pallas kernels  21.3 us (11%)
  local copies, waits for them, and re-layouts  10.1 us (5%)
    ppermute x21, waiting for transfers between devices, shifted(): return lax.ppermute(x, axis, [(i, (i + step) % 4) for i in range(4)])  64.6 us
    ppermute x21, starting transfers between devices, shifted(): return lax.ppermute(x, axis, [(i, (i + step) % 4) for i in range(4)])  37.7 us
    all_to_all x2, blocking collectives, exchange(): return lax.all_to_all(x, axes, 0, 0, tiled=True)  33.6 us
    pallas_call x7, Pallas kernels, run(): return call(*kept)  21.3 us
    all_to_all x3, starting transfers between devices, exchange(): return lax.all_to_all(x, axes, 0, 0, tiled=True)  16.5 us
    unnamed x58, local copies, waits for them, and re-layouts  8.43 us
  transfers between devices with their start and end apart: 40, of which 14 were waited for; matrix products, arithmetic and copies ran while one was open for 1% of the time, Pallas kernels for 4%

commit v1 on v0

--- a/solution.py
+++ b/solution.py
@@ -258,7 +258,7 @@
     wait_for(copies)
     for block in range(blocks):
         lanes = slice(block * width, (block + 1) * width)
-        out[block] = dot(hidden, whole[:, lanes], ((1,), (0,))).astype(bf16)
+        out[4 * (block % 4) + block // 4] = dot(hidden, whole[:, lanes], ((1,), (0,))).astype(bf16)
 
 
 def shards(
@@ -323,7 +323,8 @@
     )(core_ref, y_ref, first_branch[None], second_gain[None], tokens, tokens, second_gate, second_up)
     side = exchange(side, ("rz", "rx"))
     d1 = [shifted(d1, "rx", step) for step in (1, 2, 3)]
-    d2 = [shifted(d2, "cb", step) for step in (1, 2, 3)]
+    back, ahead = shifted(d2, "cb", 1), shifted(d2, "cb", 3)
+    d2 = [back, shifted(d2, "cb", 2), ahead]
     d1_other = [other_core(w) for w in d1]
     d2_other = [other_core(w) for w in d2]
 
@@ -382,7 +383,7 @@
         mib=24,
     )(core_ref, rows, second_down, *v1, *d2, *d2_other)
     partial, branch = lax.optimization_barrier((partial, second_branch[None]))
-    got = exchange(partial, ("rz", "rx"))
+    got = exchange(partial, ("rx", "rz"))
     out = kernel(
         finish,
         [VMEM, VMEM, HBM],

time: 190 us -> 190 us (level)
  no operation moved by 1% of the time
where the time goes in v1:
time: 190 us; the launch traced here: 189 us
  waiting for transfers between devices  66.7 us (35%)
  starting transfers between devices  57 us (30%)
  blocking collectives  33.5 us (18%)
  Pallas kernels  21.3 us (11%)
  local copies, waits for them, and re-layouts  10.1 us (5%)
    ppermute x21, waiting for transfers between devices, shifted(): return lax.ppermute(x, axis, [(i, (i + step) % 4) for i in range(4)])  64.6 us
    ppermute x21, starting transfers between devices, shifted(): return lax.ppermute(x, axis, [(i, (i + step) % 4) for i in range(4)])  37.7 us
    all_to_all x2, blocking collectives, exchange(): return lax.all_to_all(x, axes, 0, 0, tiled=True)  33.5 us
    pallas_call x7, Pallas kernels, run(): return call(*kept)  21.3 us
    all_to_all x3, starting transfers between devices, exchange(): return lax.all_to_all(x, axes, 0, 0, tiled=True)  16.5 us
    unnamed x58, local copies, waits for them, and re-layouts  8.43 us
  transfers between devices with their start and end apart: 40, of which 14 were waited for; matrix products, arithmetic and copies ran while one was open for 1% of the time, Pallas kernels for 4%

profile of v1, /device:TPU:0, one launch (start us, length us, event | category | flops | bytes accessed | tf_op | source)
XLA Modules:
  0.0 189.1 jit_solution(3616308104967625186)
XLA Ops:
  11.1 3.5 %shard_map.111 = bf16[16,112,256]{2,1,0:T(8,128)(2,1)} custom-call(s32[1]{0:T(128)} %bitcast.core_ref, s32[1]{0:T(128)} %bitcast.3.y_ref, bf16[1,256]{1,0:T(2,128)(2,1)S(1)} %broadcast_in_dim.9.branch, bf16[1,256]{1,0:T(2,128)(2,1)S(1)} %broadcast_in_dim.10.gain, bf16[512,256]{1,0:T(8,128)(2,1)} %tokens.3, bf16[512,256]{1,0:T(8,128)(2,1)} %tokens.3, ...), custom_call_target="tpu_custom_call" | custom-call | tf_op jit(solution)/shard_map/pallas_call | solution.py:299
  14.6 6.2 %all-to-all-start = ((bf16[16,112,256]{2,1,0:T(8,128)(2,1)}), bf16[16,112,256]{2,1,0:T(8,128)(2,1)S(1)}, u32[]{:S(2)}, u32[]{:S(2)}) async-start(bf16[16,112,256]{2,1,0:T(8,128)(2,1)} %shard_map.111), calls=%async_computation | async-start | bytes 1835008 | tf_op jit(solution)/shard_map/all_to_all | solution.py:19
  20.9 3.2 %collective-permute-start.2 = (bf16[512,256]{1,0:T(8,128)(2,1)S(1)}, bf16[512,256]{1,0:T(8,128)(2,1)S(1)}, u32[]{:S(2)}, u32[]{:S(2)}) collective-permute-start(bf16[512,256]{1,0:T(8,128)(2,1)S(1)} %get-tuple-element.17.first_x), channel_id=1, source_target_pairs={{0,96},{32,0},{64,32},{96,64},{1,97},{33,1},{65,33},{97,65},{2,98}... | collective-permute-start | bytes 786440 | tf_op jit(solution)/shard_map/ppermute | solution.py:27
  24.1 12.4 %collective-permute-done.4.refs_4_ = bf16[128,768]{1,0:T(8,128)(2,1)S(1)} collective-permute-done((bf16[128,768]{1,0:T(8,128)(2,1)S(1)}, bf16[128,768]{1,0:T(8,128)(2,1)S(1)}, u32[]{:S(2)}, u32[]{:S(2)}) %collective-permute-start.4) | collective-permute-done | bytes 196640 | tf_op jit(solution)/shard_map/ppermute | solution.py:27
  38.4 2.5 %collective-permute-start.13 = (bf16[96,2048]{1,0:T(8,128)(2,1)S(1)}, bf16[96,2048]{1,0:T(8,128)(2,1)S(1)}, u32[]{:S(2)}, u32[]{:S(2)}) collective-permute-start(bf16[96,2048]{1,0:T(8,128)(2,1)S(1)} %get-tuple-element.25), channel_id=1, source_target_pairs={{0,16},{8,24},{16,0},{24,8},{1,17},{9,25},{17,1},{25,9},{2,18},{10... | collective-permute-start | bytes 1179656 | tf_op jit(solution)/shard_map/ppermute | solution.py:27
  45.4 2.8 %shard_map.110 = (f32[128,768]{1,0:T(8,128)S(1)}, bf16[128,768]{1,0:T(8,128)(2,1)S(1)}, bf16[128,768]{1,0:T(8,128)(2,1)S(1)}, bf16[128,768]{1,0:T(8,128)(2,1)S(1)}) custom-call(s32[1]{0:T(128)} %bitcast.core_ref, s32[1]{0:T(128)} %bitcast.1.x_ref, s32[1]{0:T(128)} %bitcast.2.z_ref, bf16[512,256]{1,0:T(8,128)(2,1)S(1)} %get-tuple-element.17.first_x, ...), custom_call_target="tpu_custom_call" | custom-call | tf_op jit(solution)/shard_map/pallas_call | solution.py:299
  49.2 10.0 %collective-permute-done.13.refs_1_ = bf16[96,2048]{1,0:T(8,128)(2,1)S(1)} collective-permute-done((bf16[96,2048]{1,0:T(8,128)(2,1)S(1)}, bf16[96,2048]{1,0:T(8,128)(2,1)S(1)}, u32[]{:S(2)}, u32[]{:S(2)}) %collective-permute-start.13) | collective-permute-done | bytes 393248 | tf_op jit(solution)/shard_map/ppermute | solution.py:27
  63.0 2.2 %collective-permute-start.9 = (bf16[128,768]{1,0:T(8,128)(2,1)S(1)}, bf16[128,768]{1,0:T(8,128)(2,1)S(1)}, u32[]{:S(2)}, u32[]{:S(2)}) collective-permute-start(bf16[128,768]{1,0:T(8,128)(2,1)S(1)} %get-tuple-element.22), channel_id=1, source_target_pairs={{0,8},{8,16},{16,24},{24,0},{1,9},{9,17},{17,25},{25,1},{2,10},{10... | collective-permute-start | bytes 589832 | tf_op jit(solution)/shard_map/ppermute | solution.py:27
  66.7 3.8 %collective-permute-done.9.a = bf16[128,768]{1,0:T(8,128)(2,1)S(1)} collective-permute-done((bf16[128,768]{1,0:T(8,128)(2,1)S(1)}, bf16[128,768]{1,0:T(8,128)(2,1)S(1)}, u32[]{:S(2)}, u32[]{:S(2)}) %collective-permute-start.9) | collective-permute-done | bytes 196640 | tf_op jit(solution)/shard_map/ppermute | solution.py:27
  73.1 3.7 %shard_map.112 = bf16[128,4096]{1,0:T(8,128)(2,1)} custom-call(s32[1]{0:T(128)} %bitcast.core_ref, s32[1]{0:T(128)} %bitcast.1.x_ref, f32[128,768]{1,0:T(8,128)S(1)} %get-tuple-element.21.own, bf16[128,768]{1,0:T(8,128)(2,1)S(1)} %collective-permute-done.9.a, bf16[128,768]{1,0:T(8,128)(2,1)S(1)} %collective-permute-done.10.b, ...), custom_call_target="tpu_custom_call" | custom-call | tf_op jit(solution)/shard_map/pallas_call | solution.py:299
  76.8 4.7 %all-to-all-start.1 = ((bf16[16,8,4096]{2,1,0:T(8,128)(2,1)}), bf16[16,8,4096]{2,1,0:T(8,128)(2,1)S(1)}, u32[]{:S(2)}, u32[]{:S(2)}) async-start(bf16[16,8,4096]{2,1,0:T(8,128)(2,1)} %bitcast.4), calls=%async_computation.1 | async-start | bytes 2097152 | tf_op jit(solution)/shard_map/all_to_all | solution.py:19
  83.4 2.7 %collective-permute-start.32 = (bf16[96,2048]{1,0:T(8,128)(2,1)S(1)}, bf16[96,2048]{1,0:T(8,128)(2,1)S(1)}, u32[]{:S(2)}, u32[]{:S(2)}) collective-permute-start(bf16[96,2048]{1,0:T(8,128)(2,1)S(1)} %get-tuple-element.26), channel_id=1, source_target_pairs={{0,4},{2,6},{4,0},{6,2},{1,5},{3,7},{5,1},{7,3},{8,12},{10,14},{12... | collective-permute-start | bytes 1179656 | tf_op jit(solution)/shard_map/ppermute | solution.py:27
  87.6 18.1 %collective-permute-done.31.refs_14_ = bf16[96,2048]{1,0:T(8,128)(2,1)S(1)} collective-permute-done((bf16[96,2048]{1,0:T(8,128)(2,1)S(1)}, bf16[96,2048]{1,0:T(8,128)(2,1)S(1)}, u32[]{:S(2)}, u32[]{:S(2)}) %collective-permute-start.31) | collective-permute-done | bytes 393248 | tf_op jit(solution)/shard_map/ppermute | solution.py:27
  105.7 6.6 %collective-permute-done.32.refs_15_ = bf16[96,2048]{1,0:T(8,128)(2,1)S(1)} collective-permute-done((bf16[96,2048]{1,0:T(8,128)(2,1)S(1)}, bf16[96,2048]{1,0:T(8,128)(2,1)S(1)}, u32[]{:S(2)}, u32[]{:S(2)}) %collective-permute-start.32) | collective-permute-done | bytes 393248 | tf_op jit(solution)/shard_map/ppermute | solution.py:27
  113.8 3.2 %collective-permute-start.25 = (bf16[8,96,256]{2,1,0:T(8,128)(2,1)}, bf16[8,96,256]{2,1,0:T(8,128)(2,1)}, u32[]{:S(2)}, u32[]{:S(2)}) collective-permute-start(bf16[8,96,256]{2,1,0:T(8,128)(2,1)} %get-tuple-element.29), channel_id=1, source_target_pairs={{0,6},{2,0},{4,2},{6,4},{1,7},{3,1},{5,3},{7,5},{8,14},{10,8},{12,... | collective-permute-start | bytes 1179656 | tf_op jit(solution)/shard_map/ppermute | solution.py:27
  118.5 2.5 %collective-permute-start.28 = (bf16[8,96,256]{2,1,0:T(8,128)(2,1)}, bf16[8,96,256]{2,1,0:T(8,128)(2,1)}, u32[]{:S(2)}, u32[]{:S(2)}) collective-permute-start(bf16[8,96,256]{2,1,0:T(8,128)(2,1)} %get-tuple-element.30), channel_id=1, source_target_pairs={{0,6},{2,0},{4,2},{6,4},{1,7},{3,1},{5,3},{7,5},{8,14},{10,8},{12,... | collective-permute-start | bytes 1179656 | tf_op jit(solution)/shard_map/ppermute | solution.py:27
  121.0 2.2 %shard_map.113 = bf16[16,8,4352]{2,1,0:T(8,128)(2,1)} custom-call(bf16[16,8,4096]{2,1,0:T(8,128)(2,1)S(1)} %all-to-all-done.1.got, bf16[16,112,256]{2,1,0:T(8,128)(2,1)} %copy-done.2), custom_call_target="tpu_custom_call" | custom-call | tf_op jit(solution)/shard_map/pallas_call | solution.py:299
  123.2 5.5 %all-to-all-start.2 = ((bf16[16,8,4352]{2,1,0:T(8,128)(2,1)}), bf16[16,8,4352]{2,1,0:T(8,128)(2,1)S(1)}, u32[]{:S(2)}, u32[]{:S(2)}) async-start(bf16[16,8,4352]{2,1,0:T(8,128)(2,1)} %shard_map.113), calls=%async_computation.2 | async-start | bytes 2228224 | tf_op jit(solution)/shard_map/all_to_all | solution.py:19
  129.0 3.2 %collective-permute-start.26 = (bf16[8,96,256]{2,1,0:T(8,128)(2,1)}, bf16[8,96,256]{2,1,0:T(8,128)(2,1)S(1)}, u32[]{:S(2)}, u32[]{:S(2)}) collective-permute-start(bf16[8,96,256]{2,1,0:T(8,128)(2,1)} %collective-permute-done.25.refs_12_), channel_id=1, source_target_pairs={{0,6},{2,0},{4,2},{6,4},{1,7},{3,1},{5,3},{7,5},{8,14},{10,8},{12,... | collective-permute-start | bytes 1179656 | tf_op jit(solution)/shard_map/ppermute | solution.py:27
  132.2 3.5 %collective-permute-done.21.refs_4_ = bf16[8,96,256]{2,1,0:T(8,128)(2,1)} collective-permute-done((bf16[8,96,256]{2,1,0:T(8,128)(2,1)}, bf16[8,96,256]{2,1,0:T(8,128)(2,1)}, u32[]{:S(2)}, u32[]{:S(2)}) %collective-permute-start.21) | collective-permute-done | bytes 393248 | tf_op jit(solution)/shard_map/ppermute | solution.py:27
  136.2 6.9 %collective-permute-done.23.refs_6_ = bf16[8,96,256]{2,1,0:T(8,128)(2,1)S(1)} collective-permute-done((bf16[8,96,256]{2,1,0:T(8,128)(2,1)}, bf16[8,96,256]{2,1,0:T(8,128)(2,1)S(1)}, u32[]{:S(2)}, u32[]{:S(2)}) %collective-permute-start.23) | collective-permute-done | bytes 393248 | tf_op jit(solution)/shard_map/ppermute | solution.py:27
  147.2 6.7 %shard_map.114 = bf16[16,128,256]{2,1,0:T(8,128)(2,1)S(1)} custom-call(s32[1]{0:T(128)} %bitcast.core_ref, bf16[16,8,4352]{2,1,0:T(8,128)(2,1)S(1)} %all-to-all-done.2.got.send, bf16[96,4096]{1,0:T(8,128)(2,1)} %w_down.1, bf16[16,112,256]{2,1,0:T(8,128)(2,1)} %copy-done.2, bf16[16,112,256]{2,1,0:T(8,128)(2,1)S(1)} %collective-permute-done.18.refs_1_, ...), custom_call_target="tpu_custom_call" | custom-call | tf_op jit(solution)/shard_map/pallas_call | solution.py:299
  153.9 23.2 %all_to_all.25.got = bf16[16,128,256]{2,1,0:T(8,128)(2,1)S(1)} all-to-all(bf16[16,128,256]{2,1,0:T(8,128)(2,1)S(1)} %shard_map.114), channel_id=1, replica_groups=mesh['rz'=4,'rx'=4,'cb'=4,'dp'=2] {'rx','rz'}, dimensions={0} | all-to-all | bytes 2097152 | tf_op jit(solution)/shard_map/all_to_all | solution.py:19
  178.0 10.4 %all_to_all.26 = bf16[4,128,256]{2,1,0:T(8,128)(2,1)S(1)} all-to-all(bf16[4,128,256]{2,1,0:T(8,128)(2,1)S(1)} %shard_map.115), channel_id=1, replica_groups=mesh['rz'=4,'rx'=4,'cb'=4,'dp'=2] {'cb'}, dimensions={0} | all-to-all | bytes 524288 | tf_op jit(solution)/shard_map/all_to_all | solution.py:19
  (128 shorter events, 38.9 us)
Async XLA Ops:
  2.2 18.6 %collective-permute-start.3 = (bf16[128,768]{1,0:T(8,128)(2,1)S(1)}, bf16[128,768]{1,0:T(8,128)(2,1)S(1)}, u32[]{:S(2)}, u32[]{:S(2)}) collective-permute-start(bf16[128,768]{1,0:T(8,128)(2,1)S(1)} %get-tuple-element.18), channel_id=1, source_target_pairs={{0,32},{32,64},{64,96},{96,0},{1,33},{33,65},{65,97},{97,1},{2,34}... | collective-permute-start | bytes 589832 | tf_op jit(solution)/shard_map/ppermute | solution.py:27
  4.3 34.1 %collective-permute-start = (bf16[512,256]{1,0:T(8,128)(2,1)S(1)}, bf16[512,256]{1,0:T(8,128)(2,1)}, u32[]{:S(2)}, u32[]{:S(2)}) collective-permute-start(bf16[512,256]{1,0:T(8,128)(2,1)S(1)} %get-tuple-element.17.first_x), channel_id=1, source_target_pairs={{0,32},{32,64},{64,96},{96,0},{1,33},{33,65},{65,97},{97,1},{2,34}... | collective-permute-start | bytes 786440 | tf_op jit(solution)/shard_map/ppermute | solution.py:27
  6.2 34.7 %collective-permute-start.1 = (bf16[512,256]{1,0:T(8,128)(2,1)S(1)}, bf16[512,256]{1,0:T(8,128)(2,1)}, u32[]{:S(2)}, u32[]{:S(2)}) collective-permute-start(bf16[512,256]{1,0:T(8,128)(2,1)S(1)} %get-tuple-element.17.first_x), channel_id=1, source_target_pairs={{0,64},{32,96},{64,0},{96,32},{1,65},{33,97},{65,1},{97,33},{2,66}... | collective-permute-start | bytes 786440 | tf_op jit(solution)/shard_map/ppermute | solution.py:27
  8.0 28.5 %collective-permute-start.4 = (bf16[128,768]{1,0:T(8,128)(2,1)S(1)}, bf16[128,768]{1,0:T(8,128)(2,1)S(1)}, u32[]{:S(2)}, u32[]{:S(2)}) collective-permute-start(bf16[128,768]{1,0:T(8,128)(2,1)S(1)} %get-tuple-element.19), channel_id=1, source_target_pairs={{0,64},{32,96},{64,0},{96,32},{1,65},{33,97},{65,1},{97,33},{2,66}... | collective-permute-start | bytes 589832 | tf_op jit(solution)/shard_map/ppermute | solution.py:27
  9.8 26.8 %collective-permute-start.5 = (bf16[128,768]{1,0:T(8,128)(2,1)S(1)}, bf16[128,768]{1,0:T(8,128)(2,1)S(1)}, u32[]{:S(2)}, u32[]{:S(2)}) collective-permute-start(bf16[128,768]{1,0:T(8,128)(2,1)S(1)} %get-tuple-element.20), channel_id=1, source_target_pairs={{0,96},{32,0},{64,32},{96,64},{1,97},{33,1},{65,33},{97,65},{2,98}... | collective-permute-start | bytes 589832 | tf_op jit(solution)/shard_map/ppermute | solution.py:27
  14.6 57.5 %all-to-all-start = ((bf16[16,112,256]{2,1,0:T(8,128)(2,1)}), bf16[16,112,256]{2,1,0:T(8,128)(2,1)S(1)}, u32[]{:S(2)}, u32[]{:S(2)}) async-start(bf16[16,112,256]{2,1,0:T(8,128)(2,1)} %shard_map.111), calls=%async_computation | async-start | bytes 1835008 | tf_op jit(solution)/shard_map/all_to_all | solution.py:19
  20.9 21.4 %collective-permute-start.2 = (bf16[512,256]{1,0:T(8,128)(2,1)S(1)}, bf16[512,256]{1,0:T(8,128)(2,1)S(1)}, u32[]{:S(2)}, u32[]{:S(2)}) collective-permute-start(bf16[512,256]{1,0:T(8,128)(2,1)S(1)} %get-tuple-element.17.first_x), channel_id=1, source_target_pairs={{0,96},{32,0},{64,32},{96,64},{1,97},{33,1},{65,33},{97,65},{2,98}... | collective-permute-start | bytes 786440 | tf_op jit(solution)/shard_map/ppermute | solution.py:27
  38.4 20.8 %collective-permute-start.13 = (bf16[96,2048]{1,0:T(8,128)(2,1)S(1)}, bf16[96,2048]{1,0:T(8,128)(2,1)S(1)}, u32[]{:S(2)}, u32[]{:S(2)}) collective-permute-start(bf16[96,2048]{1,0:T(8,128)(2,1)S(1)} %get-tuple-element.25), channel_id=1, source_target_pairs={{0,16},{8,24},{16,0},{24,8},{1,17},{9,25},{17,1},{25,9},{2,18},{10... | collective-permute-start | bytes 1179656 | tf_op jit(solution)/shard_map/ppermute | solution.py:27
  40.9 18.4 %collective-permute-start.14 = (bf16[96,2048]{1,0:T(8,128)(2,1)S(1)}, bf16[96,2048]{1,0:T(8,128)(2,1)}, u32[]{:S(2)}, u32[]{:S(2)}) collective-permute-start(bf16[96,2048]{1,0:T(8,128)(2,1)S(1)} %get-tuple-element.25), channel_id=1, source_target_pairs={{0,24},{8,0},{16,8},{24,16},{1,25},{9,1},{17,9},{25,17},{2,26},{10... | collective-permute-start | bytes 1179656 | tf_op jit(solution)/shard_map/ppermute | solution.py:27
  48.2 14.8 %collective-permute-start.10 = (bf16[128,768]{1,0:T(8,128)(2,1)S(1)}, bf16[128,768]{1,0:T(8,128)(2,1)S(1)}, u32[]{:S(2)}, u32[]{:S(2)}) collective-permute-start(bf16[128,768]{1,0:T(8,128)(2,1)S(1)} %get-tuple-element.23), channel_id=1, source_target_pairs={{0,16},{8,24},{16,0},{24,8},{1,17},{9,25},{17,1},{25,9},{2,18},{10... | collective-permute-start | bytes 589832 | tf_op jit(solution)/shard_map/ppermute | solution.py:27
  49.2 21.3 %collective-permute-start.15 = (bf16[96,2048]{1,0:T(8,128)(2,1)S(1)}, bf16[96,2048]{1,0:T(8,128)(2,1)S(1)}, u32[]{:S(2)}, u32[]{:S(2)}) collective-permute-start(bf16[96,2048]{1,0:T(8,128)(2,1)S(1)} %collective-permute-done.12.refs_0_), channel_id=1, source_target_pairs={{0,1},{1,0},{2,3},{3,2},{4,5},{5,4},{6,7},{7,6},{8,9},{9,8},{10,11... | collective-permute-start | bytes 1179656 | tf_op jit(solution)/shard_map/ppermute | solution.py:23
  76.8 44.2 %all-to-all-start.1 = ((bf16[16,8,4096]{2,1,0:T(8,128)(2,1)}), bf16[16,8,4096]{2,1,0:T(8,128)(2,1)S(1)}, u32[]{:S(2)}, u32[]{:S(2)}) async-start(bf16[16,8,4096]{2,1,0:T(8,128)(2,1)} %bitcast.4), calls=%async_computation.1 | async-start | bytes 2097152 | tf_op jit(solution)/shard_map/all_to_all | solution.py:19
  81.5 24.2 %collective-permute-start.31 = (bf16[96,2048]{1,0:T(8,128)(2,1)S(1)}, bf16[96,2048]{1,0:T(8,128)(2,1)S(1)}, u32[]{:S(2)}, u32[]{:S(2)}) collective-permute-start(bf16[96,2048]{1,0:T(8,128)(2,1)S(1)} %get-tuple-element.26), channel_id=1, source_target_pairs={{0,2},{2,4},{4,6},{6,0},{1,3},{3,5},{5,7},{7,1},{8,10},{10,12},{12... | collective-permute-start | bytes 1179656 | tf_op jit(solution)/shard_map/ppermute | solution.py:27
  83.4 28.8 %collective-permute-start.32 = (bf16[96,2048]{1,0:T(8,128)(2,1)S(1)}, bf16[96,2048]{1,0:T(8,128)(2,1)S(1)}, u32[]{:S(2)}, u32[]{:S(2)}) collective-permute-start(bf16[96,2048]{1,0:T(8,128)(2,1)S(1)} %get-tuple-element.26), channel_id=1, source_target_pairs={{0,4},{2,6},{4,0},{6,2},{1,5},{3,7},{5,1},{7,3},{8,12},{10,14},{12... | collective-permute-start | bytes 1179656 | tf_op jit(solution)/shard_map/ppermute | solution.py:27
  86.1 26.2 %collective-permute-start.33 = (bf16[96,2048]{1,0:T(8,128)(2,1)S(1)}, bf16[96,2048]{1,0:T(8,128)(2,1)}, u32[]{:S(2)}, u32[]{:S(2)}) collective-permute-start(bf16[96,2048]{1,0:T(8,128)(2,1)S(1)} %get-tuple-element.26), channel_id=1, source_target_pairs={{0,6},{2,0},{4,2},{6,4},{1,7},{3,1},{5,3},{7,5},{8,14},{10,8},{12,... | collective-permute-start | bytes 1179656 | tf_op jit(solution)/shard_map/ppermute | solution.py:27
  112.3 16.5 %collective-permute-start.36 = (bf16[96,2048]{1,0:T(8,128)(2,1)}, bf16[96,2048]{1,0:T(8,128)(2,1)}, u32[]{:S(2)}, u32[]{:S(2)}) collective-permute-start(bf16[96,2048]{1,0:T(8,128)(2,1)} %collective-permute-done.33.refs_16_), channel_id=1, source_target_pairs={{0,1},{1,0},{2,3},{3,2},{4,5},{5,4},{6,7},{7,6},{8,9},{9,8},{10,11... | collective-permute-start | bytes 1179656 | tf_op jit(solution)/shard_map/ppermute | solution.py:23
  113.8 15.1 %collective-permute-start.19 = (bf16[8,96,256]{2,1,0:T(8,128)(2,1)}, bf16[8,96,256]{2,1,0:T(8,128)(2,1)}, u32[]{:S(2)}, u32[]{:S(2)}) collective-permute-start(bf16[8,96,256]{2,1,0:T(8,128)(2,1)} %get-tuple-element.30), channel_id=1, source_target_pairs={{0,2},{2,4},{4,6},{6,0},{1,3},{3,5},{5,7},{7,1},{8,10},{10,12},{12... | collective-permute-start | bytes 1179656 | tf_op jit(solution)/shard_map/ppermute | solution.py:27
  113.8 15.2 %collective-permute-start.25 = (bf16[8,96,256]{2,1,0:T(8,128)(2,1)}, bf16[8,96,256]{2,1,0:T(8,128)(2,1)}, u32[]{:S(2)}, u32[]{:S(2)}) collective-permute-start(bf16[8,96,256]{2,1,0:T(8,128)(2,1)} %get-tuple-element.29), channel_id=1, source_target_pairs={{0,6},{2,0},{4,2},{6,4},{1,7},{3,1},{5,3},{7,5},{8,14},{10,8},{12,... | collective-permute-start | bytes 1179656 | tf_op jit(solution)/shard_map/ppermute | solution.py:27
  117.0 18.7 %collective-permute-start.21 = (bf16[8,96,256]{2,1,0:T(8,128)(2,1)}, bf16[8,96,256]{2,1,0:T(8,128)(2,1)}, u32[]{:S(2)}, u32[]{:S(2)}) collective-permute-start(bf16[8,96,256]{2,1,0:T(8,128)(2,1)} %get-tuple-element.29), channel_id=1, source_target_pairs={{0,2},{2,4},{4,6},{6,0},{1,3},{3,5},{5,7},{7,1},{8,10},{10,12},{12... | collective-permute-start | bytes 1179656 | tf_op jit(solution)/shard_map/ppermute | solution.py:27
  118.5 17.2 %collective-permute-start.28 = (bf16[8,96,256]{2,1,0:T(8,128)(2,1)}, bf16[8,96,256]{2,1,0:T(8,128)(2,1)}, u32[]{:S(2)}, u32[]{:S(2)}) collective-permute-start(bf16[8,96,256]{2,1,0:T(8,128)(2,1)} %get-tuple-element.30), channel_id=1, source_target_pairs={{0,6},{2,0},{4,2},{6,4},{1,7},{3,1},{5,3},{7,5},{8,14},{10,8},{12,... | collective-permute-start | bytes 1179656 | tf_op jit(solution)/shard_map/ppermute | solution.py:27
  123.2 23.9 %all-to-all-start.2 = ((bf16[16,8,4352]{2,1,0:T(8,128)(2,1)}), bf16[16,8,4352]{2,1,0:T(8,128)(2,1)S(1)}, u32[]{:S(2)}, u32[]{:S(2)}) async-start(bf16[16,8,4352]{2,1,0:T(8,128)(2,1)} %shard_map.113), calls=%async_computation.2 | async-start | bytes 2228224 | tf_op jit(solution)/shard_map/all_to_all | solution.py:19
  128.8 16.9 %collective-permute-start.18 = (bf16[16,112,256]{2,1,0:T(8,128)(2,1)S(1)}, bf16[16,112,256]{2,1,0:T(8,128)(2,1)S(1)}, u32[]{:S(2)}, u32[]{:S(2)}) collective-permute-start(bf16[16,112,256]{2,1,0:T(8,128)(2,1)S(1)} %copy-done.4), channel_id=1, source_target_pairs={{0,1},{1,0},{2,3},{3,2},{4,5},{5,4},{6,7},{7,6},{8,9},{9,8},{10,11... | collective-permute-start | bytes 2752520 | tf_op jit(solution)/shard_map/ppermute | solution.py:23
  128.9 14.2 %collective-permute-start.23 = (bf16[8,96,256]{2,1,0:T(8,128)(2,1)}, bf16[8,96,256]{2,1,0:T(8,128)(2,1)S(1)}, u32[]{:S(2)}, u32[]{:S(2)}) collective-permute-start(bf16[8,96,256]{2,1,0:T(8,128)(2,1)} %collective-permute-done.19.refs_2_), channel_id=1, source_target_pairs={{0,2},{2,4},{4,6},{6,0},{1,3},{3,5},{5,7},{7,1},{8,10},{10,12},{12... | collective-permute-start | bytes 1179656 | tf_op jit(solution)/shard_map/ppermute | solution.py:27
  129.0 14.2 %collective-permute-start.26 = (bf16[8,96,256]{2,1,0:T(8,128)(2,1)}, bf16[8,96,256]{2,1,0:T(8,128)(2,1)S(1)}, u32[]{:S(2)}, u32[]{:S(2)}) collective-permute-start(bf16[8,96,256]{2,1,0:T(8,128)(2,1)} %collective-permute-done.25.refs_12_), channel_id=1, source_target_pairs={{0,6},{2,0},{4,2},{6,4},{1,7},{3,1},{5,3},{7,5},{8,14},{10,8},{12,... | collective-permute-start | bytes 1179656 | tf_op jit(solution)/shard_map/ppermute | solution.py:27
  (45 other events, 317.9 us)
